TPU v7x, 512 devices: a whole 4x4x16 slice. The times are simulated.
512 devices in a mesh: sp: 32 (over z, core), tp: 16 (over y, x).
Axes of the slice: x: 4, y: 4, z: 16, core: 2. Of those that a mesh axis runs over, the one named last changes fastest.
Arguments:
- moe_input: bfloat16 [6144, 2048], P('sp'), may hold values from -6 to 6
- out_grad: bfloat16 [6144, 2048], P('sp'), may hold values from -6 to 6
- route_ids: int32 [6144, 2], P('sp'), may hold values from 0 to 31, all different within a row; in each aligned block of 192 rows (0 to 191, 192 to 383, ...) at most 18 rows name the same one
- route_weights: float32 [6144, 2], P('sp'), may hold values from 0.2 to 2
- expert_gate: bfloat16 [32, 2048, 2048], P('sp', None, 'tp'), may hold values from -0.125 to 0.125
- expert_up: bfloat16 [32, 2048, 2048], P('sp', None, 'tp'), may hold values from -0.125 to 0.125
- expert_down: bfloat16 [32, 2048, 2048], P('sp', 'tp'), may hold values from -0.125 to 0.125
- proj_weight: bfloat16 [1024, 2048], P(None, 'tp'), may hold values from -0.1875 to 0.1875
- glu_value: bfloat16 [1024, 6144], P('tp', 'sp'), may hold values from -6 to 6
- glu_gate: bfloat16 [1024, 6144], P('tp', 'sp'), may hold values from -8 to 8
- conv_taps: float32 [1024, 31], P('tp'), may hold values from -1 to 1
- norm_input: bfloat16 [1024, 6144], P('tp', 'sp'), may hold values from -6 to 6
- norm_gain: float32 [1024], replicated, may hold values from 0.1 to 1.9
Outputs:
- grad_gate: bfloat16 [32, 2048, 2048], P('sp', None, 'tp')
- grad_up: bfloat16 [32, 2048, 2048], P('sp', None, 'tp')
- grad_down: bfloat16 [32, 2048, 2048], P('sp', 'tp')
- grad_proj: float32 [1024, 2048], P('sp', 'tp')
- grad_value: bfloat16 [1024, 6144], P('tp', 'sp')
- grad_glu_gate: bfloat16 [1024, 6144], P('tp', 'sp')
Inputs may be any that keep to these rules, and one draw needn't show every extreme that they name: `route_ids`: within the rows of one device, the 2 ids of a position differ and no expert is named by more than 18 pairs; some expert is named by exactly 18.
All inputs are finite; a program needn't handle non-finite values.
Results may differ from a plain program's by a relative error of at most 0.025.
Values may be sent and summed in bfloat16 or wider, within the bound.
No kernel may reach another device: no remote copies, remote signals or barrier semaphores. Data moves between devices by JAX's collectives and lax.ppermute only.
A program may use at most 64 MiB of HBM per device.

v0:
```python
import jax
import jax.numpy as jnp
from jax import lax
from jax.sharding import Mesh
from jax.sharding import PartitionSpec as P

TP = ("tp_0", "tp_1")
norm_eps = 1e-05


def sent_together(arrays, axis, split_dim, concat_dim, along):
    ends, at = ([], 0)
    for a in arrays[:-1]:
        at += a.shape[along]
        ends.append(at)
    both = jnp.concatenate(arrays, axis=along)
    return tuple(
        jnp.split(
            lax.all_to_all(both, axis, split_axis=split_dim, concat_axis=concat_dim, tiled=True),
            ends,
            axis=along,
        )
    )


def sent_together_2(arrays, axis, dim, along):
    ends, at = ([], 0)
    for a in arrays[:-1]:
        at += a.shape[along]
        ends.append(at)
    both = jnp.concatenate(arrays, axis=along)
    return tuple(jnp.split(lax.all_gather(both, axis, axis=dim, tiled=True), ends, axis=along))


def in_blocks(shard, dim, length):
    before, after = (shard.shape[:dim], shard.shape[dim + 1 :])
    return jnp.moveaxis(shard.reshape(*before, length, -1, *after), dim, 0)


def sum_at_owner(shard, axis, dim):
    length = lax.axis_size(axis)
    blocks = lax.all_to_all(in_blocks(shard, dim, length), axis, 0, 0, tiled=True)
    return jnp.sum(blocks.astype(jnp.float32), axis=0)


def from_everyone(shard, axis):
    length = lax.axis_size(axis)
    return lax.all_to_all(
        jnp.broadcast_to(shard[None], (length, *shard.shape)), axis, 0, 0, tiled=True
    )


def laid_out(blocks, dim):
    blocks = jnp.moveaxis(blocks, 0, dim)
    shape = blocks.shape
    return blocks.reshape(*shape[:dim], shape[dim] * shape[dim + 1], *shape[dim + 2 :])


def gather_directly(shard, axis, dim):
    blocks = from_everyone(shard, axis)
    return laid_out(blocks, dim)


def over_axes(shard, axes):
    for axis in axes:
        shard = lax.psum(shard, axis)
    return shard


def shifted(shard, axis, by):
    length = lax.axis_size(axis)
    pairs = [(i, i + by) for i in range(length) if 0 <= i + by < length]
    return lax.ppermute(shard, axis, pairs)


def silu_grad(pre):
    sigmoid_pre = jax.nn.sigmoid(pre)
    return sigmoid_pre * (1.0 + pre * (1.0 - sigmoid_pre))


def slot_table(route_ids, route_weights, experts, capacity):
    tok_rows, top_count = route_ids.shape
    flat_ids = route_ids.reshape(-1)
    onehot = (flat_ids[:, None] == jnp.arange(experts, dtype=jnp.int32)[None, :]).astype(jnp.int32)
    before = jnp.cumsum(onehot, axis=0) - onehot
    slot_index = jnp.sum(before * onehot, axis=1)
    target = flat_ids * capacity + slot_index
    buffer_rows = jnp.arange(experts * capacity, dtype=jnp.int32)
    matches = (buffer_rows[:, None] == target[None, :]).reshape(
        experts * capacity, tok_rows, top_count
    )
    placing = jnp.sum(matches.astype(jnp.float32), axis=2).astype(jnp.bfloat16)
    slot_scale = jnp.sum(jnp.where(matches, route_weights[None, :, :], 0.0), axis=(1, 2))
    return (placing, slot_scale)


def body(
    moe_input,
    out_grad,
    route_ids,
    route_weights,
    expert_gate,
    expert_up,
    expert_down,
    proj_weight,
    glu_value,
    glu_gate,
    conv_taps,
    norm_input,
    norm_gain,
):
    groups = lax.axis_size("sp")
    lane_count = lax.axis_size(TP)
    lane_index = lax.axis_index(TP)
    tok_rows, model_width = moe_input.shape
    top_count = route_ids.shape[1]
    capacity = tok_rows * top_count * 3 // (2 * groups)
    part_width = model_width // lane_count
    placing, slot_scale = slot_table(route_ids, route_weights, groups, capacity)
    own_grad = lax.dynamic_slice_in_dim(out_grad, lane_index * part_width, part_width, 1)
    own_input = lax.dynamic_slice_in_dim(moe_input, lane_index * part_width, part_width, 1)
    sent_rows = jnp.dot(placing, own_input, preferred_element_type=jnp.float32).astype(jnp.bfloat16)
    sent_grad = (
        jnp.dot(placing, own_grad, preferred_element_type=jnp.float32) * slot_scale[:, None]
    ).astype(jnp.bfloat16)
    part_rows, part_grad = sent_together(
        (
            sent_rows.reshape(groups, capacity, part_width),
            sent_grad.reshape(groups, capacity, part_width),
        ),
        "sp",
        0,
        0,
        1,
    )
    arrived_rows, arrived_grad = sent_together_2((part_rows, part_grad), TP, 2, 0)
    token_rows = arrived_rows.reshape(-1, model_width)
    grad_rows = arrived_grad.reshape(-1, model_width)
    w_gate = expert_gate[0]
    w_up = expert_up[0]
    w_down = expert_down[0]
    gate_pre = jnp.dot(token_rows, w_gate, preferred_element_type=jnp.float32)
    up_pre = jnp.dot(token_rows, w_up, preferred_element_type=jnp.float32)
    gate_act = jax.nn.silu(gate_pre)
    hidden = (gate_act * up_pre).astype(jnp.bfloat16)
    down_grad = lax.dot_general(
        hidden, grad_rows, (((0,), (0,)), ((), ())), preferred_element_type=jnp.float32
    ).astype(jnp.bfloat16)
    grad_hidden = lax.dot_general(
        grad_rows, w_down, (((1,), (1,)), ((), ())), preferred_element_type=jnp.float32
    )
    gate_grad = (grad_hidden * up_pre * silu_grad(gate_pre)).astype(jnp.bfloat16)
    up_grad = (grad_hidden * gate_act).astype(jnp.bfloat16)
    gate_wgrad = lax.dot_general(
        token_rows, gate_grad, (((0,), (0,)), ((), ())), preferred_element_type=jnp.float32
    ).astype(jnp.bfloat16)
    up_wgrad = lax.dot_general(
        token_rows, up_grad, (((0,), (0,)), ((), ())), preferred_element_type=jnp.float32
    ).astype(jnp.bfloat16)
    input_grad = lax.dot_general(
        gate_grad, w_gate, (((1,), (1,)), ((), ())), preferred_element_type=jnp.float32
    )
    input_grad = input_grad + lax.dot_general(
        up_grad, w_up, (((1,), (1,)), ((), ())), preferred_element_type=jnp.float32
    )
    summed_grad = sum_at_owner(input_grad.astype(jnp.bfloat16), TP, 1).astype(jnp.bfloat16)
    returned = lax.all_to_all(
        summed_grad.reshape(groups, capacity, part_width),
        "sp",
        split_axis=0,
        concat_axis=0,
        tiled=True,
    )
    moe_grad = lax.dot_general(
        placing,
        returned.reshape(-1, part_width),
        (((0,), (0,)), ((), ())),
        preferred_element_type=jnp.float32,
    )
    mix_grad = (own_grad.astype(jnp.float32) + moe_grad).astype(jnp.bfloat16)
    channel_part = norm_input.shape[0]
    conv_values = gather_directly(norm_input, TP, 0).astype(jnp.float32)
    channels = conv_values.shape[0]
    centred = conv_values - jnp.mean(conv_values, axis=0, keepdims=True)
    inv_scale = lax.rsqrt(jnp.mean(centred * centred, axis=0, keepdims=True) + norm_eps)
    normed = centred * inv_scale
    scaled = normed * norm_gain[:, None]
    act = jax.nn.silu(scaled).astype(jnp.bfloat16)
    grad_proj = sum_at_owner(
        jnp.dot(act, mix_grad, preferred_element_type=jnp.float32).astype(jnp.bfloat16), "sp", 0
    )
    act_partial = lax.dot_general(
        proj_weight, mix_grad, (((1,), (1,)), ((), ())), preferred_element_type=jnp.float32
    )
    grad_act = sum_at_owner(act_partial.astype(jnp.bfloat16), TP, 0)
    normed_own = lax.dynamic_slice_in_dim(normed, lane_index * channel_part, channel_part, 0)
    scaled_own = lax.dynamic_slice_in_dim(scaled, lane_index * channel_part, channel_part, 0)
    gain_own = lax.dynamic_slice_in_dim(norm_gain, lane_index * channel_part, channel_part, 0)
    grad_normed = grad_act * silu_grad(scaled_own) * gain_own[:, None]
    sum_grad, sum_cross = (
        over_axes(jnp.sum(grad_normed, axis=0), TP),
        over_axes(jnp.sum(grad_normed * normed_own, axis=0), TP),
    )
    grad_conv = inv_scale * (
        grad_normed - sum_grad[None, :] / channels - normed_own * (sum_cross[None, :] / channels)
    )
    taps_count = conv_taps.shape[1]
    reach_back = taps_count - 1
    ahead_rows = shifted(grad_conv[:, :reach_back], "sp", -1)
    extended = jnp.concatenate([grad_conv, ahead_rows], axis=1)
    grad_glu = jnp.zeros_like(grad_conv)
    for tap_index in range(taps_count):
        grad_glu = (
            grad_glu
            + conv_taps[:, tap_index : tap_index + 1]
            * extended[:, reach_back - tap_index : reach_back - tap_index + tok_rows]
        )
    sigmoid_gate = jax.nn.sigmoid(glu_gate.astype(jnp.float32))
    grad_value = (grad_glu * sigmoid_gate).astype(jnp.bfloat16)
    grad_glu_gate = (
        grad_glu * glu_value.astype(jnp.float32) * sigmoid_gate * (1.0 - sigmoid_gate)
    ).astype(jnp.bfloat16)
    return (gate_wgrad[None], up_wgrad[None], down_grad[None], grad_proj, grad_value, grad_glu_gate)


def solution(mesh):
    finer = Mesh(mesh.devices.reshape(mesh.shape["sp"], 4, 4), ("sp", "tp_0", "tp_1"))
    return jax.shard_map(
        body,
        mesh=finer,
        in_specs=(
            P("sp", None),
            P("sp", None),
            P("sp", None),
            P("sp", None),
            P("sp", None, TP),
            P("sp", None, TP),
            P("sp", TP, None),
            P(None, TP),
            P(TP, "sp"),
            P(TP, "sp"),
            P(TP, None),
            P(TP, "sp"),
            P(),
        ),
        out_specs=(
            P("sp", None, TP),
            P("sp", None, TP),
            P("sp", TP, None),
            P("sp", TP),
            P(TP, "sp"),
            P(TP, "sp"),
        ),
        check_vma=False,
    )
```

profile of v0, /device:TPU:1, one launch (start us, length us, event | category | flops | bytes accessed | tf_op | source)
XLA Modules:
  0.0 290.6 jit_solution(6470165151364125645)
XLA Ops:
  13.1 41.5 %all_to_all.30 = bf16[32,36,128]{2,1,0:T(8,128)(2,1)S(1)} all-to-all(bf16[32,36,128]{2,1,0:T(8,128)(2,1)S(1)} %pad_maximum_fusion.1), channel_id=1, replica_groups=mesh['sp'=32,'tp_0'=4,'tp_1'=4] {'sp'}, dimensions={0} | all-to-all | bytes 589824 | tf_op jit(solution)/shard_map/all_to_all | solution.py:19
  56.4 6.8 %all-to-all-start.1 = ((bf16[16,64,192]{2,1,0:T(8,128)(2,1)}), bf16[16,64,192]{2,1,0:T(8,128)(2,1)}, u32[]{:S(2)}, u32[]{:S(2)}) async-start(bf16[16,64,192]{2,1,0:T(8,128)(2,1)} %broadcast_in_dim.25), calls=%async_computation.1 | async-start | bytes 1048576 | tf_op jit(solution)/shard_map/all_to_all | solution.py:48
  63.2 64.7 %all-gather.2.cloned.1.call-done = bf16[64,18,2048]{2,1,0:T(8,128)(2,1)} async-done(((bf16[64,18,128]{2,1,0:T(8,128)(2,1)}), bf16[64,18,2048]{2,1,0:T(8,128)(2,1)}) %all-gather.2.cloned.1.call-update) | async-done | bytes 4718608 | tf_op jit(solution)/shard_map/all_gather | solution.py:32
  128.0 6.6 %fusion.123 = (bf16[32,18,2048]{2,1,0:T(8,128)(2,1)}, bf16[32,18,2048]{2,1,0:T(8,128)(2,1)}) fusion(bf16[64,18,2048]{2,1,0:T(8,128)(2,1)} %all-gather.2.cloned.1.call-done), kind=kLoop, calls=%fused_computation.232 | loop fusion | bytes 9437184 | tf_op jit(solution)/shard_map/split | solution.py:32
  134.6 2.9 %reshape.106 = bf16[576,2048]{1,0:T(8,128)(2,1)S(1)} reshape(bf16[32,18,2048]{2,1,0:T(8,128)(2,1)} %get-tuple-element.18) | data formatting | bytes 4718592 | tf_op jit(solution)/shard_map/reshape | solution.py:137
  137.5 2.6 fusion.10
  140.1 1.5 fusion.13
  141.6 4.3 %reshape.107 = bf16[576,2048]{1,0:T(8,128)(2,1)} reshape(bf16[32,18,2048]{2,1,0:T(8,128)(2,1)} %get-tuple-element.17) | data formatting | bytes 4718592 | tf_op jit(solution)/shard_map/reshape | solution.py:138
  145.9 2.8 multiply_convert_fusion.3
  150.6 2.1 copy.54
  152.7 4.8 %all-to-all-start.2 = ((bf16[16,576,128]{2,1,0:T(8,128)(2,1)}), bf16[16,576,128]{2,1,0:T(8,128)(2,1)}, u32[]{:S(2)}, u32[]{:S(2)}) async-start(bf16[16,576,128]{2,1,0:T(8,128)(2,1)} %bitcast.138), calls=%async_computation.2 | async-start | bytes 4718592 | tf_op jit(solution)/shard_map/all_to_all | solution.py:42
  159.5 1.2 convert_reduce_fusion.2
  160.7 1.2 multiply_reduce_fusion
  161.9 26.0 %all-to-all-done.2 = bf16[16,576,128]{2,1,0:T(8,128)(2,1)} async-done(((bf16[16,576,128]{2,1,0:T(8,128)(2,1)}), bf16[16,576,128]{2,1,0:T(8,128)(2,1)}, u32[]{:S(2)}, u32[]{:S(2)}) %all-to-all-start.2) | async-done | bytes 2359328 | tf_op jit(solution)/shard_map/all_to_all | solution.py:42
  188.0 2.0 reduce_sum.101
  190.7 16.8 %all-to-all-start.3 = ((bf16[32,18,128]{2,1,0:T(8,128)(2,1)}), bf16[32,18,128]{2,1,0:T(8,128)(2,1)}, u32[]{:S(2)}, u32[]{:S(2)}) async-start(bf16[32,18,128]{2,1,0:T(8,128)(2,1)} %reshape.109), calls=%async_computation.3 | async-start | bytes 393216 | tf_op jit(solution)/shard_map/all_to_all | solution.py:167
  208.1 2.7 fusion.7
  210.8 2.5 fusion.2
  213.3 13.1 %all-to-all-done.3 = bf16[32,18,128]{2,1,0:T(8,128)(2,1)} async-done(((bf16[32,18,128]{2,1,0:T(8,128)(2,1)}), bf16[32,18,128]{2,1,0:T(8,128)(2,1)}, u32[]{:S(2)}, u32[]{:S(2)}) %all-to-all-start.3) | async-done | bytes 147488 | tf_op jit(solution)/shard_map/all_to_all | solution.py:167
  229.0 1.2 fusion.4
  231.2 4.4 %all-to-all-start.5 = ((bf16[16,64,192]{2,1,0:T(8,128)(2,1)}), bf16[16,64,192]{2,1,0:T(8,128)(2,1)}, u32[]{:S(2)}, u32[]{:S(2)}) async-start(bf16[16,64,192]{2,1,0:T(8,128)(2,1)} %bitcast.139), calls=%async_computation.5 | async-start | bytes 1048576 | tf_op jit(solution)/shard_map/all_to_all | solution.py:42
  235.7 2.7 fusion
  239.5 6.2 %all-to-all-done.5 = bf16[16,64,192]{2,1,0:T(8,128)(2,1)} async-done(((bf16[16,64,192]{2,1,0:T(8,128)(2,1)}), bf16[16,64,192]{2,1,0:T(8,128)(2,1)}, u32[]{:S(2)}, u32[]{:S(2)}) %all-to-all-start.5) | async-done | bytes 393248 | tf_op jit(solution)/shard_map/all_to_all | solution.py:42
  245.7 5.8 %all-to-all-start.4 = ((bf16[32,32,128]{2,1,0:T(8,128)(2,1)}), bf16[32,32,128]{2,1,0:T(8,128)(2,1)S(1)}, u32[]{:S(2)}, u32[]{:S(2)}) async-start(bf16[32,32,128]{2,1,0:T(8,128)(2,1)} %bitcast.140), calls=%async_computation.4 | async-start | bytes 524288 | tf_op jit(solution)/shard_map/all_to_all | solution.py:42
  251.5 1.1 convert_reduce_fusion
  252.6 2.2 fusion.121
  254.8 7.8 %all-reduce.1 = (f32[192]{0:T(256)}, f32[192]{0:T(256)}) all-reduce(f32[192]{0:T(256)} %get-tuple-element.7, f32[192]{0:T(256)} %get-tuple-element.6), channel_id=1, replica_groups=mesh['sp'=32,'tp_0'=4,'tp_1'=4] {'tp_0'}, use_global_device_ids=true, to_apply=%region_14.15 | all-reduce | flops 384 | bytes 3072 | tf_op jit(solution)/shard_map/psum | solution.py:66
  262.6 7.6 %all-reduce = (f32[192]{0:T(256)}, f32[192]{0:T(256)}) all-reduce(f32[192]{0:T(256)} %get-tuple-element.12, f32[192]{0:T(256)} %get-tuple-element.13), channel_id=1, replica_groups=mesh['sp'=32,'tp_0'=4,'tp_1'=4] {'tp_1'}, use_global_device_ids=true, to_apply=%region_15.16 | all-reduce | flops 384 | bytes 3072 | tf_op jit(solution)/shard_map/psum | solution.py:66
  272.1 5.4 %collective-permute-start = (f32[64,30]{1,0:T(8,128)S(1)}, f32[64,30]{1,0:T(8,128)S(1)}, u32[]{:S(2)}, u32[]{:S(2)}) collective-permute-start(f32[64,30]{1,0:T(8,128)S(1)} %slice.257), channel_id=1, source_target_pairs={{16,0},{32,16},{48,32},{64,48},{80,64},{96,80},{112,96},{128,112},... | collective-permute-start | bytes 23048 | tf_op jit(solution)/shard_map/ppermute | solution.py:73
  277.5 1.7 fusion.1
  279.2 1.2 collective-permute-done
  280.7 1.8 multiply_convert_fusion.6
  (137 shorter events, 20.5 us)
Async XLA Ops:
  7.2 120.8 %all-gather.2.cloned.1.call-start = ((), (), s32[]{:S(2)}) async-start(), calls=%async_computation.6 | async-start | bytes 6684672 | tf_op jit(solution)/shard_map/all_gather | solution.py:32
  11.5 44.0 %copy-start.12 = (bf16[64,192]{1,0:T(8,128)(2,1)S(1)}, bf16[64,192]{1,0:T(8,128)(2,1)}, u32[]{:S(2)}) copy-start(bf16[64,192]{1,0:T(8,128)(2,1)} %param.24) | copy-start | bytes 73732
  56.4 96.3 %all-to-all-start.1 = ((bf16[16,64,192]{2,1,0:T(8,128)(2,1)}), bf16[16,64,192]{2,1,0:T(8,128)(2,1)}, u32[]{:S(2)}, u32[]{:S(2)}) async-start(bf16[16,64,192]{2,1,0:T(8,128)(2,1)} %broadcast_in_dim.25), calls=%async_computation.1 | async-start | bytes 1048576 | tf_op jit(solution)/shard_map/all_to_all | solution.py:48
  152.7 35.3 %all-to-all-start.2 = ((bf16[16,576,128]{2,1,0:T(8,128)(2,1)}), bf16[16,576,128]{2,1,0:T(8,128)(2,1)}, u32[]{:S(2)}, u32[]{:S(2)}) async-start(bf16[16,576,128]{2,1,0:T(8,128)(2,1)} %bitcast.138), calls=%async_computation.2 | async-start | bytes 4718592 | tf_op jit(solution)/shard_map/all_to_all | solution.py:42
  190.7 35.7 %all-to-all-start.3 = ((bf16[32,18,128]{2,1,0:T(8,128)(2,1)}), bf16[32,18,128]{2,1,0:T(8,128)(2,1)}, u32[]{:S(2)}, u32[]{:S(2)}) async-start(bf16[32,18,128]{2,1,0:T(8,128)(2,1)} %reshape.109), calls=%async_computation.3 | async-start | bytes 393216 | tf_op jit(solution)/shard_map/all_to_all | solution.py:167
  231.2 14.5 %all-to-all-start.5 = ((bf16[16,64,192]{2,1,0:T(8,128)(2,1)}), bf16[16,64,192]{2,1,0:T(8,128)(2,1)}, u32[]{:S(2)}, u32[]{:S(2)}) async-start(bf16[16,64,192]{2,1,0:T(8,128)(2,1)} %bitcast.139), calls=%async_computation.5 | async-start | bytes 1048576 | tf_op jit(solution)/shard_map/all_to_all | solution.py:42
  238.4 39.1 %copy-start.7 = (bf16[576,128]{1,0:T(8,128)(2,1)S(1)}, bf16[576,128]{1,0:T(8,128)(2,1)}, u32[]{:S(2)}) copy-start(bf16[576,128]{1,0:T(8,128)(2,1)} %copy-done.6) | copy-start | bytes 442372
  245.7 37.4 %all-to-all-start.4 = ((bf16[32,32,128]{2,1,0:T(8,128)(2,1)}), bf16[32,32,128]{2,1,0:T(8,128)(2,1)S(1)}, u32[]{:S(2)}, u32[]{:S(2)}) async-start(bf16[32,32,128]{2,1,0:T(8,128)(2,1)} %bitcast.140), calls=%async_computation.4 | async-start | bytes 524288 | tf_op jit(solution)/shard_map/all_to_all | solution.py:42
  271.7 8.6 %copy-start.11 = (bf16[64,192]{1,0:T(8,128)(2,1)S(1)}, bf16[64,192]{1,0:T(8,128)(2,1)}, u32[]{:S(2)}) copy-start(bf16[64,192]{1,0:T(8,128)(2,1)} %param.22) | copy-start | bytes 73732
  271.7 8.6 %copy-start.13 = (bf16[64,192]{1,0:T(8,128)(2,1)S(1)}, bf16[64,192]{1,0:T(8,128)(2,1)}, u32[]{:S(2)}) copy-start(bf16[64,192]{1,0:T(8,128)(2,1)} %param.21) | copy-start | bytes 73732
  271.8 8.6 %copy-start.17 = (f32[64]{0:T(128)S(1)}, f32[64]{0:T(128)}, u32[]{:S(2)}) copy-start(f32[64]{0:T(128)} %get-tuple-element.44) | copy-start | bytes 772
  271.8 8.6 %copy-start.18 = (f32[64]{0:T(128)S(1)}, f32[64]{0:T(128)}, u32[]{:S(2)}) copy-start(f32[64]{0:T(128)} %get-tuple-element.45) | copy-start | bytes 772
  271.8 8.6 %copy-start.19 = (f32[64]{0:T(128)S(1)}, f32[64]{0:T(128)}, u32[]{:S(2)}) copy-start(f32[64]{0:T(128)} %get-tuple-element.46) | copy-start | bytes 772
  271.8 8.6 %copy-start.20 = (f32[64]{0:T(128)S(1)}, f32[64]{0:T(128)}, u32[]{:S(2)}) copy-start(f32[64]{0:T(128)} %get-tuple-element.47) | copy-start | bytes 772
  271.8 8.6 %copy-start.21 = (f32[64]{0:T(128)S(1)}, f32[64]{0:T(128)}, u32[]{:S(2)}) copy-start(f32[64]{0:T(128)} %get-tuple-element.48) | copy-start | bytes 772
  271.8 8.6 %copy-start.22 = (f32[64]{0:T(128)S(1)}, f32[64]{0:T(128)}, u32[]{:S(2)}) copy-start(f32[64]{0:T(128)} %get-tuple-element.49) | copy-start | bytes 772
  271.8 8.6 %copy-start.23 = (f32[64]{0:T(128)S(1)}, f32[64]{0:T(128)}, u32[]{:S(2)}) copy-start(f32[64]{0:T(128)} %get-tuple-element.50) | copy-start | bytes 772
  271.8 8.6 %copy-start.24 = (f32[64]{0:T(128)S(1)}, f32[64]{0:T(128)}, u32[]{:S(2)}) copy-start(f32[64]{0:T(128)} %get-tuple-element.51) | copy-start | bytes 772
  271.8 8.6 %copy-start.25 = (f32[64]{0:T(128)S(1)}, f32[64]{0:T(128)}, u32[]{:S(2)}) copy-start(f32[64]{0:T(128)} %get-tuple-element.52) | copy-start | bytes 772
  271.8 8.6 %copy-start.26 = (f32[64]{0:T(128)S(1)}, f32[64]{0:T(128)}, u32[]{:S(2)}) copy-start(f32[64]{0:T(128)} %get-tuple-element.53) | copy-start | bytes 772
  271.9 8.6 %copy-start.27 = (f32[64]{0:T(128)S(1)}, f32[64]{0:T(128)}, u32[]{:S(2)}) copy-start(f32[64]{0:T(128)} %get-tuple-element.54) | copy-start | bytes 772
  271.9 8.6 %copy-start.28 = (f32[64]{0:T(128)S(1)}, f32[64]{0:T(128)}, u32[]{:S(2)}) copy-start(f32[64]{0:T(128)} %get-tuple-element.55) | copy-start | bytes 772
  271.9 8.6 %copy-start.29 = (f32[64]{0:T(128)S(1)}, f32[64]{0:T(128)}, u32[]{:S(2)}) copy-start(f32[64]{0:T(128)} %get-tuple-element.25) | copy-start | bytes 772
  271.9 8.6 %copy-start.30 = (f32[64]{0:T(128)S(1)}, f32[64]{0:T(128)}, u32[]{:S(2)}) copy-start(f32[64]{0:T(128)} %get-tuple-element.26) | copy-start | bytes 772
  271.9 8.6 %copy-start.31 = (f32[64]{0:T(128)S(1)}, f32[64]{0:T(128)}, u32[]{:S(2)}) copy-start(f32[64]{0:T(128)} %get-tuple-element.27) | copy-start | bytes 772
  271.9 8.6 %copy-start.32 = (f32[64]{0:T(128)S(1)}, f32[64]{0:T(128)}, u32[]{:S(2)}) copy-start(f32[64]{0:T(128)} %get-tuple-element.28) | copy-start | bytes 772
  271.9 8.6 %copy-start.33 = (f32[64]{0:T(128)S(1)}, f32[64]{0:T(128)}, u32[]{:S(2)}) copy-start(f32[64]{0:T(128)} %get-tuple-element.29) | copy-start | bytes 772
  271.9 8.6 %copy-start.34 = (f32[64]{0:T(128)S(1)}, f32[64]{0:T(128)}, u32[]{:S(2)}) copy-start(f32[64]{0:T(128)} %get-tuple-element.30) | copy-start | bytes 772
  271.9 8.6 %copy-start.35 = (f32[64]{0:T(128)S(1)}, f32[64]{0:T(128)}, u32[]{:S(2)}) copy-start(f32[64]{0:T(128)} %get-tuple-element.31) | copy-start | bytes 772
  271.9 8.6 %copy-start.36 = (f32[64]{0:T(128)S(1)}, f32[64]{0:T(128)}, u32[]{:S(2)}) copy-start(f32[64]{0:T(128)} %get-tuple-element.32) | copy-start | bytes 772
  272.0 8.6 %copy-start.37 = (f32[64]{0:T(128)S(1)}, f32[64]{0:T(128)}, u32[]{:S(2)}) copy-start(f32[64]{0:T(128)} %get-tuple-element.33) | copy-start | bytes 772
  272.1 8.3 %collective-permute-start = (f32[64,30]{1,0:T(8,128)S(1)}, f32[64,30]{1,0:T(8,128)S(1)}, u32[]{:S(2)}, u32[]{:S(2)}) collective-permute-start(f32[64,30]{1,0:T(8,128)S(1)} %slice.257), channel_id=1, source_target_pairs={{16,0},{32,16},{48,32},{64,48},{80,64},{96,80},{112,96},{128,112},... | collective-permute-start | bytes 23048 | tf_op jit(solution)/shard_map/ppermute | solution.py:73
  (23 other events, 120.1 us)
Sparse Core Ops, SparseCore 0:
  55.7 72.2 all-gather.1
where the time goes:
time: 292 us; the launch traced here: 291 us
  waiting for transfers between devices  111 us (38%)
  blocking collectives  56.9 us (19%)
  starting transfers between devices  44.1 us (15%)
  local copies, waits for them, and re-layouts  24.8 us (8%)
  matrix products  20 us (7%)
  other arithmetic  18.6 us (6%)
  between operations  14.9 us (5%)
    all_gather x1, waiting for transfers between devices, sent_together_2(): lax.all_gather(both, axis, axis=dim, tiled=True)  64.7 us
    all_to_all x1, blocking collectives, sent_together(): lax.all_to_all(both, axis, split_axis=split_dim, concat_axis=concat_dim,...  41.5 us
    all_to_all x3, waiting for transfers between devices, sum_at_owner(): lax.all_to_all(in_blocks(shard, dim, length), axis, 0, 0, tiled=True)  32.2 us
    all_to_all x1, starting transfers between devices, body(): lax.all_to_all(summed_grad.reshape(groups, capacity, part_width), 'sp', s...  16.8 us
    psum x2, blocking collectives, over_axes(): shard = lax.psum(shard, axis)  15.4 us
    all_to_all x3, starting transfers between devices, sum_at_owner(): lax.all_to_all(in_blocks(shard, dim, length), axis, 0, 0, tiled=True)  15 us
    all_to_all x1, waiting for transfers between devices, body(): lax.all_to_all(summed_grad.reshape(groups, capacity, part_width), 'sp', s...  13.1 us
    all_to_all x1, starting transfers between devices, from_everyone(): lax.all_to_all(jnp.broadcast_to(shard[None], (length, *shard.shape)), axi...  6.81 us
  transfers between devices with their start and end apart: 7, of which 5 were waited for; matrix products, arithmetic and copies ran while one was open for 16% of the time, Pallas kernels for 0%

commit v1 on v0

--- a/solution.py
+++ b/solution.py
@@ -63,7 +63,10 @@
 
 def over_axes(shard, axes):
     for axis in axes:
-        shard = lax.psum(shard, axis)
+        recover_the_keys = lambda payload, mesh_dim: jnp.sum(
+            lax.all_gather(payload, axis_name=mesh_dim), axis=0
+        )
+        shard = recover_the_keys(shard, axis)
     return shard
 
 

time: 292 us -> 311 us (1.065)
  local copies, waits for them, and re-layouts: 24.8 us -> 40.6 us
  other arithmetic: 18.6 us -> 23.7 us
  waiting for transfers between devices: 111 us -> 107 us
    psum x2 -> x0, blocking collectives: 15.4 us -> none  [over_axes(): shard = lax.psum(shard, axis)]
    unnamed x0 -> x2, blocking collectives: none -> 15.3 us
    unnamed x97 -> x107, local copies, waits for them, and re-layouts: 2.54 us -> 13 us
    all_gather x0 -> x4, local copies, waits for them, and re-layouts: none -> 5.42 us  [over_axes(): lax.all_gather(payload, axis_name=mesh_dim)]
    reduce_sum x0 -> x4, other arithmetic: none -> 5.06 us  [over_axes(): jnp.sum(lax.all_gather(payload, axis_name=mesh_dim), axis=0)]
    all_to_all x3, waiting for transfers between devices: 32.2 us -> 28.4 us  [sum_at_owner(): lax.all_to_all(in_blocks(shard, dim, length), axis, 0, 0, tiled=True)]
  transfers between devices with their start and end apart: 7 -> 7, of which waited for: 5 -> 5; matrix products, arithmetic and copies ran while one was open for 16% -> 22% of each run, Pallas kernels for 0% -> 0%
where the time goes in v1:
time: 311 us; the launch traced here: 309 us
  waiting for transfers between devices  107 us (34%)
  blocking collectives  56.8 us (18%)
  starting transfers between devices  44.4 us (14%)
  local copies, waits for them, and re-layouts  40.6 us (13%)
  other arithmetic  23.7 us (8%)
  matrix products  20 us (6%)
  between operations  16.2 us (5%)
    all_gather x1, waiting for transfers between devices, sent_together_2(): lax.all_gather(both, axis, axis=dim, tiled=True)  64.7 us
    all_to_all x1, blocking collectives, sent_together(): lax.all_to_all(both, axis, split_axis=split_dim, concat_axis=concat_dim,...  41.5 us
    all_to_all x3, waiting for transfers between devices, sum_at_owner(): lax.all_to_all(in_blocks(shard, dim, length), axis, 0, 0, tiled=True)  28.4 us
    all_to_all x1, starting transfers between devices, body(): lax.all_to_all(summed_grad.reshape(groups, capacity, part_width), 'sp', s...  16.8 us
    unnamed x2, blocking collectives  15.3 us
    all_to_all x3, starting transfers between devices, sum_at_owner(): lax.all_to_all(in_blocks(shard, dim, length), axis, 0, 0, tiled=True)  15 us
    all_to_all x1, waiting for transfers between devices, body(): lax.all_to_all(summed_grad.reshape(groups, capacity, part_width), 'sp', s...  13.1 us
    unnamed x107, local copies, waits for them, and re-layouts  13 us
  transfers between devices with their start and end apart: 7, of which 5 were waited for; matrix products, arithmetic and copies ran while one was open for 22% of the time, Pallas kernels for 0%

profile of v1, /device:TPU:1, one launch (start us, length us, event | category | flops | bytes accessed | tf_op | source)
XLA Modules:
  0.0 309.2 jit_solution(10044723152118392922)
XLA Ops:
  13.1 41.5 %all_to_all.30 = bf16[32,36,128]{2,1,0:T(8,128)(2,1)S(1)} all-to-all(bf16[32,36,128]{2,1,0:T(8,128)(2,1)S(1)} %pad_maximum_fusion.1), channel_id=1, replica_groups=mesh['sp'=32,'tp_0'=4,'tp_1'=4] {'sp'}, dimensions={0} | all-to-all | bytes 589824 | tf_op jit(solution)/shard_map/all_to_all | solution.py:19
  56.4 6.8 %all-to-all-start.1 = ((bf16[16,64,192]{2,1,0:T(8,128)(2,1)}), bf16[16,64,192]{2,1,0:T(8,128)(2,1)}, u32[]{:S(2)}, u32[]{:S(2)}) async-start(bf16[16,64,192]{2,1,0:T(8,128)(2,1)} %broadcast_in_dim.25), calls=%async_computation.1 | async-start | bytes 1048576 | tf_op jit(solution)/shard_map/all_to_all | solution.py:48
  63.2 64.7 %all-gather.6.cloned.1.call-done = bf16[64,18,2048]{2,1,0:T(8,128)(2,1)} async-done(((bf16[64,18,128]{2,1,0:T(8,128)(2,1)}), bf16[64,18,2048]{2,1,0:T(8,128)(2,1)}) %all-gather.6.cloned.1.call-update) | async-done | bytes 4718608 | tf_op jit(solution)/shard_map/all_gather | solution.py:32
  128.0 6.6 %fusion.123 = (bf16[32,18,2048]{2,1,0:T(8,128)(2,1)}, bf16[32,18,2048]{2,1,0:T(8,128)(2,1)}) fusion(bf16[64,18,2048]{2,1,0:T(8,128)(2,1)} %all-gather.6.cloned.1.call-done), kind=kLoop, calls=%fused_computation.232 | loop fusion | bytes 9437184 | tf_op jit(solution)/shard_map/split | solution.py:32
  134.6 2.9 reshape.110
  137.5 2.6 fusion.10
  140.1 1.5 fusion.13
  141.6 4.3 %reshape.111 = bf16[576,2048]{1,0:T(8,128)(2,1)} reshape(bf16[32,18,2048]{2,1,0:T(8,128)(2,1)} %get-tuple-element.17) | data formatting | bytes 4718592 | tf_op jit(solution)/shard_map/reshape | solution.py:141
  145.9 2.8 multiply_convert_fusion.3
  150.7 2.1 copy.54
  152.7 4.8 %all-to-all-start.2 = ((bf16[16,576,128]{2,1,0:T(8,128)(2,1)}), bf16[16,576,128]{2,1,0:T(8,128)(2,1)}, u32[]{:S(2)}, u32[]{:S(2)}) async-start(bf16[16,576,128]{2,1,0:T(8,128)(2,1)} %bitcast.140), calls=%async_computation.2 | async-start | bytes 4718592 | tf_op jit(solution)/shard_map/all_to_all | solution.py:42
  165.8 22.2 %all-to-all-done.2 = bf16[16,576,128]{2,1,0:T(8,128)(2,1)} async-done(((bf16[16,576,128]{2,1,0:T(8,128)(2,1)}), bf16[16,576,128]{2,1,0:T(8,128)(2,1)}, u32[]{:S(2)}, u32[]{:S(2)}) %all-to-all-start.2) | async-done | bytes 2359328 | tf_op jit(solution)/shard_map/all_to_all | solution.py:42
  188.0 2.0 reduce_sum.137
  190.7 16.8 %all-to-all-start.3 = ((bf16[32,18,128]{2,1,0:T(8,128)(2,1)}), bf16[32,18,128]{2,1,0:T(8,128)(2,1)}, u32[]{:S(2)}, u32[]{:S(2)}) async-start(bf16[32,18,128]{2,1,0:T(8,128)(2,1)} %reshape.113), calls=%async_computation.3 | async-start | bytes 393216 | tf_op jit(solution)/shard_map/all_to_all | solution.py:170
  208.2 2.6 fusion.7
  210.8 2.5 fusion.2
  213.3 13.1 %all-to-all-done.3 = bf16[32,18,128]{2,1,0:T(8,128)(2,1)} async-done(((bf16[32,18,128]{2,1,0:T(8,128)(2,1)}), bf16[32,18,128]{2,1,0:T(8,128)(2,1)}, u32[]{:S(2)}, u32[]{:S(2)}) %all-to-all-start.3) | async-done | bytes 147488 | tf_op jit(solution)/shard_map/all_to_all | solution.py:170
  231.2 4.4 %all-to-all-start.5 = ((bf16[16,64,192]{2,1,0:T(8,128)(2,1)}), bf16[16,64,192]{2,1,0:T(8,128)(2,1)}, u32[]{:S(2)}, u32[]{:S(2)}) async-start(bf16[16,64,192]{2,1,0:T(8,128)(2,1)} %bitcast.141), calls=%async_computation.5 | async-start | bytes 1048576 | tf_op jit(solution)/shard_map/all_to_all | solution.py:42
  235.7 2.7 fusion
  239.5 6.2 %all-to-all-done.5 = bf16[16,64,192]{2,1,0:T(8,128)(2,1)} async-done(((bf16[16,64,192]{2,1,0:T(8,128)(2,1)}), bf16[16,64,192]{2,1,0:T(8,128)(2,1)}, u32[]{:S(2)}, u32[]{:S(2)}) %all-to-all-start.5) | async-done | bytes 393248 | tf_op jit(solution)/shard_map/all_to_all | solution.py:42
  245.7 5.8 %all-to-all-start.4 = ((bf16[32,32,128]{2,1,0:T(8,128)(2,1)}), bf16[32,32,128]{2,1,0:T(8,128)(2,1)S(1)}, u32[]{:S(2)}, u32[]{:S(2)}) async-start(bf16[32,32,128]{2,1,0:T(8,128)(2,1)} %bitcast.142), calls=%async_computation.4 | async-start | bytes 524288 | tf_op jit(solution)/shard_map/all_to_all | solution.py:42
  252.6 2.2 fusion.121
  255.4 1.4 dynamic-update-slice.2
  257.4 1.4 dynamic-update-slice
  258.7 7.9 %all-reduce.5 = (f32[768]{0:T(1024)}, f32[768]{0:T(1024)}) all-reduce(f32[768]{0:T(1024)} %dynamic-update-slice.2, f32[768]{0:T(1024)} %dynamic-update-slice), channel_id=4, replica_groups=mesh['sp'=32,'tp_0'=4,'tp_1'=4] {'tp_0'}, use_global_device_ids=true, to_apply=%add.2 | all-reduce | flops 1536 | bytes 12288
  268.0 1.4 reshape.118
  272.5 1.4 dynamic-update-slice.3
  274.5 1.4 dynamic-update-slice.1
  275.8 7.4 %all-reduce.4 = (f32[768]{0:T(1024)}, f32[768]{0:T(1024)}) all-reduce(f32[768]{0:T(1024)} %dynamic-update-slice.3, f32[768]{0:T(1024)} %dynamic-update-slice.1), channel_id=5, replica_groups=mesh['sp'=32,'tp_0'=4,'tp_1'=4] {'tp_1'}, use_global_device_ids=true, to_apply=%add.3 | all-reduce | flops 1536 | bytes 12288
  290.4 5.7 %collective-permute-start = (f32[64,30]{1,0:T(8,128)S(1)}, f32[64,30]{1,0:T(8,128)S(1)}, u32[]{:S(2)}, u32[]{:S(2)}) collective-permute-start(f32[64,30]{1,0:T(8,128)S(1)} %slice.257), channel_id=1, source_target_pairs={{16,0},{32,16},{48,32},{64,48},{80,64},{96,80},{112,96},{128,112},... | collective-permute-start | bytes 23048 | tf_op jit(solution)/shard_map/ppermute | solution.py:76
  296.1 1.7 fusion.1
  299.3 1.8 multiply_convert_fusion.6
  (155 shorter events, 40.4 us)
Async XLA Ops:
  7.2 120.8 %all-gather.6.cloned.1.call-start = ((), (), s32[]{:S(2)}) async-start(), calls=%async_computation.6 | async-start | bytes 6684672 | tf_op jit(solution)/shard_map/all_gather | solution.py:32
  11.5 44.0 %copy-start.12 = (bf16[64,192]{1,0:T(8,128)(2,1)S(1)}, bf16[64,192]{1,0:T(8,128)(2,1)}, u32[]{:S(2)}) copy-start(bf16[64,192]{1,0:T(8,128)(2,1)} %param.24) | copy-start | bytes 73732
  56.4 96.3 %all-to-all-start.1 = ((bf16[16,64,192]{2,1,0:T(8,128)(2,1)}), bf16[16,64,192]{2,1,0:T(8,128)(2,1)}, u32[]{:S(2)}, u32[]{:S(2)}) async-start(bf16[16,64,192]{2,1,0:T(8,128)(2,1)} %broadcast_in_dim.25), calls=%async_computation.1 | async-start | bytes 1048576 | tf_op jit(solution)/shard_map/all_to_all | solution.py:48
  152.7 9.3 %copy-start.14 = (f32[64,31]{0,1:T(8,128)S(1)}, f32[64,31]{0,1:T(8,128)}, u32[]{:S(2)}) copy-start(f32[64,31]{0,1:T(8,128)} %param.23) | copy-start | bytes 23812
  152.7 35.3 %all-to-all-start.2 = ((bf16[16,576,128]{2,1,0:T(8,128)(2,1)}), bf16[16,576,128]{2,1,0:T(8,128)(2,1)}, u32[]{:S(2)}, u32[]{:S(2)}) async-start(bf16[16,576,128]{2,1,0:T(8,128)(2,1)} %bitcast.140), calls=%async_computation.2 | async-start | bytes 4718592 | tf_op jit(solution)/shard_map/all_to_all | solution.py:42
  190.7 35.7 %all-to-all-start.3 = ((bf16[32,18,128]{2,1,0:T(8,128)(2,1)}), bf16[32,18,128]{2,1,0:T(8,128)(2,1)}, u32[]{:S(2)}, u32[]{:S(2)}) async-start(bf16[32,18,128]{2,1,0:T(8,128)(2,1)} %reshape.113), calls=%async_computation.3 | async-start | bytes 393216 | tf_op jit(solution)/shard_map/all_to_all | solution.py:170
  231.2 14.5 %all-to-all-start.5 = ((bf16[16,64,192]{2,1,0:T(8,128)(2,1)}), bf16[16,64,192]{2,1,0:T(8,128)(2,1)}, u32[]{:S(2)}, u32[]{:S(2)}) async-start(bf16[16,64,192]{2,1,0:T(8,128)(2,1)} %bitcast.141), calls=%async_computation.5 | async-start | bytes 1048576 | tf_op jit(solution)/shard_map/all_to_all | solution.py:42
  238.4 57.7 %copy-start.7 = (bf16[576,128]{1,0:T(8,128)(2,1)S(1)}, bf16[576,128]{1,0:T(8,128)(2,1)}, u32[]{:S(2)}) copy-start(bf16[576,128]{1,0:T(8,128)(2,1)} %copy-done.6) | copy-start | bytes 442372
  245.7 56.0 %all-to-all-start.4 = ((bf16[32,32,128]{2,1,0:T(8,128)(2,1)}), bf16[32,32,128]{2,1,0:T(8,128)(2,1)S(1)}, u32[]{:S(2)}, u32[]{:S(2)}) async-start(bf16[32,32,128]{2,1,0:T(8,128)(2,1)} %bitcast.142), calls=%async_computation.4 | async-start | bytes 524288 | tf_op jit(solution)/shard_map/all_to_all | solution.py:42
  290.1 8.9 %copy-start.11 = (bf16[64,192]{1,0:T(8,128)(2,1)S(1)}, bf16[64,192]{1,0:T(8,128)(2,1)}, u32[]{:S(2)}) copy-start(bf16[64,192]{1,0:T(8,128)(2,1)} %param.22) | copy-start | bytes 73732
  290.1 8.9 %copy-start.13 = (bf16[64,192]{1,0:T(8,128)(2,1)S(1)}, bf16[64,192]{1,0:T(8,128)(2,1)}, u32[]{:S(2)}) copy-start(bf16[64,192]{1,0:T(8,128)(2,1)} %param.21) | copy-start | bytes 73732
  290.1 8.9 %copy-start.17 = (f32[64]{0:T(128)S(1)}, f32[64]{0:T(128)}, u32[]{:S(2)}) copy-start(f32[64]{0:T(128)} %get-tuple-element.44) | copy-start | bytes 772
  290.1 8.9 %copy-start.18 = (f32[64]{0:T(128)S(1)}, f32[64]{0:T(128)}, u32[]{:S(2)}) copy-start(f32[64]{0:T(128)} %get-tuple-element.45) | copy-start | bytes 772
  290.1 8.9 %copy-start.19 = (f32[64]{0:T(128)S(1)}, f32[64]{0:T(128)}, u32[]{:S(2)}) copy-start(f32[64]{0:T(128)} %get-tuple-element.46) | copy-start | bytes 772
  290.1 8.9 %copy-start.20 = (f32[64]{0:T(128)S(1)}, f32[64]{0:T(128)}, u32[]{:S(2)}) copy-start(f32[64]{0:T(128)} %get-tuple-element.47) | copy-start | bytes 772
  290.1 8.9 %copy-start.21 = (f32[64]{0:T(128)S(1)}, f32[64]{0:T(128)}, u32[]{:S(2)}) copy-start(f32[64]{0:T(128)} %get-tuple-element.48) | copy-start | bytes 772
  290.1 8.9 %copy-start.22 = (f32[64]{0:T(128)S(1)}, f32[64]{0:T(128)}, u32[]{:S(2)}) copy-start(f32[64]{0:T(128)} %get-tuple-element.49) | copy-start | bytes 772
  290.1 8.9 %copy-start.23 = (f32[64]{0:T(128)S(1)}, f32[64]{0:T(128)}, u32[]{:S(2)}) copy-start(f32[64]{0:T(128)} %get-tuple-element.50) | copy-start | bytes 772
  290.2 8.9 %copy-start.24 = (f32[64]{0:T(128)S(1)}, f32[64]{0:T(128)}, u32[]{:S(2)}) copy-start(f32[64]{0:T(128)} %get-tuple-element.51) | copy-start | bytes 772
  290.2 8.9 %copy-start.25 = (f32[64]{0:T(128)S(1)}, f32[64]{0:T(128)}, u32[]{:S(2)}) copy-start(f32[64]{0:T(128)} %get-tuple-element.52) | copy-start | bytes 772
  290.2 8.9 %copy-start.26 = (f32[64]{0:T(128)S(1)}, f32[64]{0:T(128)}, u32[]{:S(2)}) copy-start(f32[64]{0:T(128)} %get-tuple-element.53) | copy-start | bytes 772
  290.2 8.9 %copy-start.27 = (f32[64]{0:T(128)S(1)}, f32[64]{0:T(128)}, u32[]{:S(2)}) copy-start(f32[64]{0:T(128)} %get-tuple-element.54) | copy-start | bytes 772
  290.2 8.9 %copy-start.28 = (f32[64]{0:T(128)S(1)}, f32[64]{0:T(128)}, u32[]{:S(2)}) copy-start(f32[64]{0:T(128)} %get-tuple-element.55) | copy-start | bytes 772
  290.2 8.9 %copy-start.29 = (f32[64]{0:T(128)S(1)}, f32[64]{0:T(128)}, u32[]{:S(2)}) copy-start(f32[64]{0:T(128)} %get-tuple-element.25) | copy-start | bytes 772
  290.2 8.9 %copy-start.30 = (f32[64]{0:T(128)S(1)}, f32[64]{0:T(128)}, u32[]{:S(2)}) copy-start(f32[64]{0:T(128)} %get-tuple-element.26) | copy-start | bytes 772
  290.2 8.9 %copy-start.31 = (f32[64]{0:T(128)S(1)}, f32[64]{0:T(128)}, u32[]{:S(2)}) copy-start(f32[64]{0:T(128)} %get-tuple-element.27) | copy-start | bytes 772
  290.2 8.9 %copy-start.32 = (f32[64]{0:T(128)S(1)}, f32[64]{0:T(128)}, u32[]{:S(2)}) copy-start(f32[64]{0:T(128)} %get-tuple-element.28) | copy-start | bytes 772
  290.2 8.9 %copy-start.33 = (f32[64]{0:T(128)S(1)}, f32[64]{0:T(128)}, u32[]{:S(2)}) copy-start(f32[64]{0:T(128)} %get-tuple-element.29) | copy-start | bytes 772
  290.3 8.9 %copy-start.34 = (f32[64]{0:T(128)S(1)}, f32[64]{0:T(128)}, u32[]{:S(2)}) copy-start(f32[64]{0:T(128)} %get-tuple-element.30) | copy-start | bytes 772
  290.3 8.9 %copy-start.35 = (f32[64]{0:T(128)S(1)}, f32[64]{0:T(128)}, u32[]{:S(2)}) copy-start(f32[64]{0:T(128)} %get-tuple-element.31) | copy-start | bytes 772
  290.3 8.9 %copy-start.36 = (f32[64]{0:T(128)S(1)}, f32[64]{0:T(128)}, u32[]{:S(2)}) copy-start(f32[64]{0:T(128)} %get-tuple-element.32) | copy-start | bytes 772
  290.4 8.6 %collective-permute-start = (f32[64,30]{1,0:T(8,128)S(1)}, f32[64,30]{1,0:T(8,128)S(1)}, u32[]{:S(2)}, u32[]{:S(2)}) collective-permute-start(f32[64,30]{1,0:T(8,128)S(1)} %slice.257), channel_id=1, source_target_pairs={{16,0},{32,16},{48,32},{64,48},{80,64},{96,80},{112,96},{128,112},... | collective-permute-start | bytes 23048 | tf_op jit(solution)/shard_map/ppermute | solution.py:76
  (23 other events, 130.3 us)
Sparse Core Ops, SparseCore 0:
  55.7 72.2 all-gather.5
